TPU v7x, 256 devices: a whole 4x4x8 slice. The times are simulated.
256 devices in a mesh: sp: 64 (over z, y, core), tp: 4 (over x).
Axes of the slice: x: 4, y: 4, z: 8, core: 2. Of those that a mesh axis runs over, the one named last changes fastest.
Arguments:
- layer_grad: bfloat16 [12288, 2048], P('sp'), may hold values from -16 to 16
- routes: int32 [12288, 2], P('sp'), may hold values from 0 to 63, as said below
- route_weight: float32 [12288, 2], P('sp'), may hold values from 0.1 to 0.9
- slot_tokens: bfloat16 [64, 576, 2048], P('sp'), may hold values from -6 to 6
- gate_proj: bfloat16 [64, 2048, 1024], P('sp', None, 'tp'), may hold values from -0.125 to 0.125
- up_proj: bfloat16 [64, 2048, 1024], P('sp', None, 'tp'), may hold values from -0.125 to 0.125
- down_proj: bfloat16 [64, 1024, 2048], P('sp', 'tp'), may hold values from -0.1875 to 0.1875
- out_proj: bfloat16 [2048, 1024], P(None, 'tp'), may hold values from -0.1875 to 0.1875
- queries: bfloat16 [12288, 512], P('sp', 'tp'), may hold values from -6 to 6
- keys: bfloat16 [12288, 512], P('sp', 'tp'), may hold values from -6 to 6
- values: bfloat16 [12288, 1024], P('sp', 'tp'), may hold values from -6 to 6
- fwd_decay: float32 [12288, 512], P('sp', 'tp'), may hold values from -2 to 0
- bwd_decay: float32 [12288, 512], P('sp', 'tp'), may hold values from -2 to 0
Outputs:
- gate_grad: bfloat16 [64, 2048, 1024], P('sp', None, 'tp')
- up_grad: bfloat16 [64, 2048, 1024], P('sp', None, 'tp')
- down_grad: bfloat16 [64, 1024, 2048], P('sp', 'tp')
- proj_grad: float32 [2048, 1024], P('sp', 'tp')
- query_grad: bfloat16 [12288, 512], P('sp', 'tp')
- key_grad: bfloat16 [12288, 512], P('sp', 'tp')
- value_grad: bfloat16 [12288, 1024], P('sp', 'tp')
Inputs may be any that keep to these rules, and one draw needn't show every extreme that they name: `routes`: each row names two different experts of one group of 8 consecutive experts. In every aligned block of 192 rows one expert is named by 9 rows or more.
All inputs are finite; a program needn't handle non-finite values.
Results may differ from a plain program's by a relative error of at most 0.015.
Values may be sent and summed in bfloat16 or wider, within the bound.
A program may use at most 128 MiB of HBM per device.

v0:
```python
import jax
import jax.numpy as jnp
from jax import lax
from jax.sharding import Mesh
from jax.sharding import PartitionSpec as P

KEY_CHANNELS = 64
DV = 128
BLOCK = 64
SP = ("sp_0", "sp_1", "sp_2")
EPSILON = 1e-06


def filled_with(array, identity):
    return jax.tree.map(
        lambda a, e: jnp.broadcast_to(jnp.asarray(e, a.dtype), a.shape), array, identity
    )


def all_in_one(array, axis):
    leaves = jax.tree.leaves(array)
    sequence = sorted(range(len(leaves)), key=lambda k: -leaves[k].size)
    width = (1, *leaves[sequence[0]].shape)[-1]
    lines = [
        jnp.pad(leaves[k].reshape(-1), (0, -leaves[k].size % width)).reshape(-1, width)
        for k in sequence
    ]
    both, at, found = (lax.all_gather(jnp.concatenate(lines), axis), 0, {})
    for k, line in zip(sequence, lines):
        slab = both[:, at : at + len(line)].reshape(len(both), -1)
        found[k] = slab[:, : leaves[k].size].reshape(-1, *leaves[k].shape)
        at += len(line)
    numbers = iter(range(len(leaves)))
    return jax.tree.map(lambda _: found[next(numbers)], array)


def once_a_type(array, axis):
    leaves, found = (jax.tree.leaves(array), {})
    for leading, a in enumerate(leaves):
        if leading not in found:
            alike = [k for k, b in enumerate(leaves) if b.dtype == a.dtype]
            got = (
                all_in_one([leaves[k] for k in alike], axis)
                if len(alike) > 1
                else [lax.all_gather(a, axis)]
            )
            for k, b in zip(alike, got):
                found[k] = b
    numbers = iter(range(len(leaves)))
    return jax.tree.map(lambda _: found[next(numbers)], array)


def carried_in(array, axes, combine, identity, reverse):
    before = start = filled_with(array, identity)
    total = array
    for axis in reversed(axes):
        devices, index = (lax.axis_size(axis), lax.axis_index(axis))
        pieces = once_a_type(total, axis)
        inside, total = (start, start)
        for k in reversed(range(devices)) if reverse else range(devices):
            passed = k > index if reverse else k < index
            total = combine(total, jax.tree.map(lambda part: part[k], pieces))
            inside = jax.tree.map(lambda new, old: jnp.where(passed, new, old), total, inside)
        before = combine(inside, before)
    return before


def copy_for_each(array, axis):
    devices = lax.axis_size(axis)
    return lax.all_to_all(
        jnp.broadcast_to(array[None], (devices, *array.shape)), axis, 0, 0, tiled=True
    )


def in_order(pieces, dim):
    shape = list(pieces.shape[1:])
    shape[dim] *= pieces.shape[0]
    return jnp.moveaxis(pieces, 0, dim).reshape(shape)


def gathered_copies(array, axis, dim):
    pieces = copy_for_each(array, axis)
    return in_order(pieces, dim)


def split_up(array, dim, devices):
    before, after = (array.shape[:dim], array.shape[dim + 1 :])
    return jnp.moveaxis(array.reshape(*before, devices, -1, *after), dim, 0)


def sum_at_owner(array, axis, dim):
    pieces = split_up(array, dim, lax.axis_size(axis))
    arrived = lax.all_to_all(pieces, axis, split_axis=0, concat_axis=0, tiled=True)
    return arrived.sum(axis=0)


def sweep(query_rows, keyrows, valrows, log_decay, strict):
    nheads, length, kwidth = query_rows.shape
    vwidth = valrows.shape[-1]
    number = length // BLOCK
    offset = -1 if strict else 0
    causal = jnp.tril(jnp.ones((BLOCK, BLOCK), jnp.float32), offset)

    def split(array):
        return jnp.moveaxis(array.reshape(nheads, number, BLOCK, array.shape[-1]), 1, 0)

    def advance(carried_state, pieces):
        query_block, key_block, value_block, gblock = pieces
        running_total = jnp.cumsum(gblock, axis=1)
        middle = running_total[:, BLOCK // 2 - 1 : BLOCK // 2, :]
        scores = (
            jnp.einsum(
                "hik,hjk->hij",
                query_block * jnp.exp(running_total - middle),
                key_block * jnp.exp(middle - running_total),
            )
            * causal
        )
        inner = jnp.einsum("hij,hjv->hiv", scores, value_block)
        outer_product = jnp.einsum(
            "zuw,zwo->zuo", query_block * jnp.exp(running_total), carried_state
        )
        final_row = running_total[:, -1:, :]
        fresh_state = jnp.einsum(
            "xor,xot->xrt", key_block * jnp.exp(final_row - running_total), value_block
        )
        return (
            jnp.exp(final_row[:, 0, :])[:, :, None] * carried_state + fresh_state,
            inner + outer_product,
        )

    start_state = jnp.zeros((nheads, kwidth, vwidth), jnp.float32)
    final, outputs = lax.scan(
        advance, start_state, (split(query_rows), split(keyrows), split(valrows), split(log_decay))
    )
    return (jnp.moveaxis(outputs, 0, 1).reshape(nheads, length, vwidth), final)


def slot_ranks(expert_ids, experts):
    members = (expert_ids[:, None] == jnp.arange(experts, dtype=jnp.int32)[None, :]).astype(
        jnp.int32
    )
    before = jnp.cumsum(members, axis=0) - members
    return jnp.sum(before * members, axis=1)


def local_pass(query_rows, keyrows, valrows, fwd_log, bwd_log):
    forward_out, forward_end = sweep(query_rows, keyrows, valrows, fwd_log, False)
    backward_out, backward_end = sweep(
        jnp.flip(query_rows, 1),
        jnp.flip(keyrows, 1),
        jnp.flip(valrows, 1),
        jnp.flip(bwd_log, 1),
        True,
    )
    return (forward_out, forward_end, jnp.flip(backward_out, 1), backward_end)


def finish(query_rows, fwd_log, bwd_log, forward_out, backward_out, forward_entry, backward_entry):
    rising_decay = jnp.exp(jnp.cumsum(fwd_log, axis=1))
    falling_decay = jnp.exp(jnp.flip(jnp.cumsum(jnp.flip(bwd_log, 1), axis=1), 1))
    mixed = forward_out + backward_out
    mixed = mixed + jnp.einsum("xfj,xji->xfi", query_rows * rising_decay, forward_entry)
    mixed = mixed + jnp.einsum("xfj,xji->xfi", query_rows * falling_decay, backward_entry)
    return mixed * lax.rsqrt(jnp.mean(mixed * mixed, axis=-1, keepdims=True) + EPSILON)


def combine(earlier, later):
    return (earlier[0] * later[0], later[0][:, :, None] * earlier[1] + later[1])


def carry(decays, terms, backward):
    identity = (jnp.ones_like(decays), jnp.zeros_like(terms))
    return carried_in((decays, terms), SP, combine, identity, backward)[1]


def on_device(
    layer_grad,
    routes,
    route_weight,
    slot_tokens,
    gate_proj,
    up_proj,
    down_proj,
    out_proj,
    queries,
    keys,
    values,
    fwd_decay,
    bwd_decay,
):
    devices = lax.axis_size(SP)
    rows_here = layer_grad.shape[0]
    width = layer_grad.shape[1]
    slots = slot_tokens.shape[1]
    capacity = slots // devices
    expert_ids = routes.reshape(-1)
    ranks = slot_ranks(expert_ids, devices)
    kept = ranks < capacity
    target = jnp.where(kept, expert_ids * capacity + ranks, slots)
    sender = (
        jnp.full((slots + 1,), -1, jnp.int32)
        .at[target]
        .set(jnp.arange(2 * rows_here, dtype=jnp.int32))[:slots]
    )
    anchor = jnp.maximum(sender, 0)
    scaled = route_weight.reshape(-1)[anchor] * (sender >= 0).astype(jnp.float32)
    column_share = width // lax.axis_size("tp")
    own_slice = lax.dynamic_slice_in_dim(
        layer_grad, lax.axis_index("tp") * column_share, column_share, 1
    )
    outgoing = (own_slice[anchor // 2].astype(jnp.float32) * scaled[:, None]).astype(jnp.bfloat16)
    arrived = lax.all_to_all(
        outgoing.reshape(devices, capacity, column_share),
        SP,
        split_axis=0,
        concat_axis=0,
        tiled=True,
    ).reshape(slots, column_share)
    inbound = gathered_copies(arrived, "tp", 1)
    inputs = slot_tokens[0]
    w_gate = gate_proj[0]
    w_upper = up_proj[0]
    w_down = down_proj[0]
    gate = jnp.dot(inputs, w_gate, preferred_element_type=jnp.float32)
    upper = jnp.dot(inputs, w_upper, preferred_element_type=jnp.float32)
    sigma = jax.nn.sigmoid(gate)
    act = (gate * sigma * upper).astype(jnp.bfloat16)
    grad_down = lax.dot_general(
        act, inbound, (((0,), (0,)), ((), ())), preferred_element_type=jnp.float32
    )
    act_grad = lax.dot_general(
        inbound, w_down, (((1,), (1,)), ((), ())), preferred_element_type=jnp.float32
    )
    up_delta = (act_grad * gate * sigma).astype(jnp.bfloat16)
    gate_delta = (act_grad * upper * sigma * (1.0 + gate * (1.0 - sigma))).astype(jnp.bfloat16)
    grad_gate = lax.dot_general(
        inputs, gate_delta, (((0,), (0,)), ((), ())), preferred_element_type=jnp.float32
    )
    grad_up = lax.dot_general(
        inputs, up_delta, (((0,), (0,)), ((), ())), preferred_element_type=jnp.float32
    )
    slot_part = lax.dot_general(
        gate_delta, w_gate, (((1,), (1,)), ((), ())), preferred_element_type=jnp.float32
    )
    slot_part = slot_part + lax.dot_general(
        up_delta, w_upper, (((1,), (1,)), ((), ())), preferred_element_type=jnp.float32
    )
    safe_target = jnp.minimum(target, slots - 1)
    kept_float = kept.astype(jnp.float32)[:, None]
    quarter = width // lax.axis_size("tp")
    summed = lax.psum_scatter(slot_part.astype(jnp.bfloat16), "tp", scatter_dimension=1, tiled=True)
    backrows = lax.all_to_all(
        summed.reshape(devices, capacity, quarter), SP, split_axis=0, concat_axis=0, tiled=True
    ).reshape(slots, quarter)
    picked = backrows[safe_target].astype(jnp.float32) * kept_float
    moe_grad = jnp.sum(picked.reshape(rows_here, 2, quarter), axis=1)
    own_columns = lax.dynamic_slice_in_dim(layer_grad, lax.axis_index("tp") * quarter, quarter, 1)
    stream_part = (own_columns.astype(jnp.float32) + moe_grad).astype(jnp.bfloat16)
    stream_grad = lax.all_gather(stream_part, "tp", axis=1, tiled=True)
    scale = KEY_CHANNELS ** (-0.5)

    def split_heads(array, size):
        return array.astype(jnp.float32).reshape(rows_here, -1, size).transpose(1, 0, 2)

    def merge_heads(array):
        return array.transpose(1, 0, 2).reshape(rows_here, -1)

    query_heads = split_heads(queries, KEY_CHANNELS) * scale
    fwd_heads = split_heads(fwd_decay, KEY_CHANNELS)
    bwd_heads = split_heads(bwd_decay, KEY_CHANNELS)
    local_out, local_pull = jax.vjp(
        local_pass,
        query_heads,
        split_heads(keys, KEY_CHANNELS),
        split_heads(values, DV),
        fwd_heads,
        bwd_heads,
    )
    forward_out, forward_end, backward_out, backward_end = local_out
    fwd_total = jnp.exp(jnp.sum(fwd_heads, axis=1))
    bwd_total = jnp.exp(jnp.sum(bwd_heads, axis=1))
    forward_entry = carry(fwd_total, forward_end, False)
    backward_entry = carry(bwd_total, backward_end, True)
    mixed, finish_pull = jax.vjp(
        finish,
        query_heads,
        fwd_heads,
        bwd_heads,
        forward_out,
        backward_out,
        forward_entry,
        backward_entry,
    )
    mixed_rows = merge_heads(mixed).astype(jnp.bfloat16)
    proj_grad = sum_at_owner(
        lax.dot_general(
            stream_grad, mixed_rows, (((0,), (0,)), ((), ())), preferred_element_type=jnp.float32
        ),
        SP,
        0,
    )
    mixed_grad = jnp.dot(stream_grad, out_proj, preferred_element_type=jnp.float32)
    query_first, fwd_first, bwd_first, forward_cot, backward_cot, fwd_direct, bwd_direct = (
        finish_pull(split_heads(mixed_grad, DV))
    )
    fwd_after = carry(fwd_total, fwd_direct, True)
    bwd_after = carry(bwd_total, bwd_direct, False)
    query_second, key_part, value_part, fwd_unused, bwd_unused = local_pull(
        (forward_cot, fwd_after, backward_cot, bwd_after)
    )
    query_grad = (merge_heads(query_first + query_second) * scale).astype(jnp.bfloat16)
    return (
        grad_gate.astype(jnp.bfloat16)[None],
        grad_up.astype(jnp.bfloat16)[None],
        grad_down.astype(jnp.bfloat16)[None],
        proj_grad,
        query_grad,
        merge_heads(key_part).astype(jnp.bfloat16),
        merge_heads(value_part).astype(jnp.bfloat16),
    )


def solution(mesh):
    torus = Mesh(mesh.devices.reshape(8, 4, 2, mesh.shape["tp"]), ("sp_0", "sp_1", "sp_2", "tp"))
    in_specs = (
        P(SP, None),
        P(SP, None),
        P(SP, None),
        P(SP, None, None),
        P(SP, None, "tp"),
        P(SP, None, "tp"),
        P(SP, "tp", None),
        P(None, "tp"),
        P(SP, "tp"),
        P(SP, "tp"),
        P(SP, "tp"),
        P(SP, "tp"),
        P(SP, "tp"),
    )
    out_specs = (
        P(SP, None, "tp"),
        P(SP, None, "tp"),
        P(SP, "tp", None),
        P(SP, "tp"),
        P(SP, "tp"),
        P(SP, "tp"),
        P(SP, "tp"),
    )
    return jax.shard_map(
        on_device, mesh=torus, in_specs=in_specs, out_specs=out_specs, check_vma=False
    )
```

profile of v0, /device:TPU:1, one launch (start us, length us, event | category | flops | bytes accessed | tf_op | source)
XLA Modules:
  0.0 496.6 jit_solution(14228876233473937465)
XLA Ops:
  11.3 2.9 scatter_custom_fusion
  15.2 2.7 gather_fusion
  19.8 4.0 gather_fusion.1
  23.9 2.8 multiply_convert_fusion
  26.7 13.5 %all-to-all-start = ((bf16[64,9,512]{2,1,0:T(8,128)(2,1)}), bf16[64,9,512]{2,1,0:T(8,128)(2,1)}, u32[]{:S(2)}, u32[]{:S(2)}) async-start(bf16[64,9,512]{2,1,0:T(8,128)(2,1)} %multiply_convert_fusion), calls=%async_computation | async-start | bytes 2097152 | tf_op jit(solution)/shard_map/all_to_all | solution.py:213
  57.9 17.1 %while.115 = (s32[]{:T(128)}, f32[2,64,128]{2,1,0:T(8,128)S(1)}, f32[3,2,64,128]{3,2,1,0:T(8,128)}, f32[3,2,64,64]{3,2,1,0:T(8,128)}, f32[3,2,64,64]{3,2,1,0:T(8...) while((s32[]{:T(128)}, f32[2,64,128]{2,1,0:T(8,128)S(1)}, ...), condition=%wide.region_11.12_spmd.clone, body=%wide.region_9.11_spmd.clone.sunk | while | flops 8093699 | bytes 2081263 | solution.py:133
  82.1 12.8 %while.114 = (s32[]{:T(128)}, f32[2,64,128]{2,1,0:T(8,128)S(1)}, f32[3,2,64,128]{3,2,1,0:T(8,128)}, f32[3,2,64,64]{3,2,1,0:T(8,128)}, f32[3,2,64,64]{3,2,1,0:T(8...) while((s32[]{:T(128)}, f32[2,64,128]{2,1,0:T(8,128)S(1)}, ...), condition=%wide.region_8.9_spmd.clone, body=%wide.region_6.8_spmd.clone.sunk | while | flops 8093699 | bytes 1981671 | solution.py:133
  100.8 2.1 all-gather.12
  103.1 10.3 %all-gather.13 = f32[4,129,128]{2,1,0:T(8,128)S(1)} all-gather(f32[1,129,128]{2,1,0:T(8,128)S(1)} %maximum_bitcast_fusion), channel_id=3, replica_groups=mesh['sp_0'=8,'sp_1'=4,'sp_2'=2,'tp'=4] {'sp_1'}, dimensions={0}, use_global_device_ids=true | all-gather | bytes 330240 | tf_op jit(solution)/shard_map/all_gather | solution.py:28
  118.3 4.6 all-to-all-start.1
  123.0 4.2 all-gather.15
  127.9 10.8 %all-gather.16 = f32[4,129,128]{2,1,0:T(8,128)S(1)} all-gather(f32[1,129,128]{2,1,0:T(8,128)S(1)} %maximum_bitcast_fusion.2), channel_id=6, replica_groups=mesh['sp_0'=8,'sp_1'=4,'sp_2'=2,'tp'=4] {'sp_1'}, dimensions={0}, use_global_device_ids=true | all-gather | bytes 330240 | tf_op jit(solution)/shard_map/all_gather | solution.py:28
  139.4 2.9 fusion.175
  144.0 5.6 %all-to-all-done.1 = bf16[4,576,512]{2,1,0:T(8,128)(2,1)} async-done(((bf16[4,576,512]{2,1,0:T(8,128)(2,1)}), bf16[4,576,512]{2,1,0:T(8,128)(2,1)}, u32[]{:S(2)}, u32[]{:S(2)}) %all-to-all-start.1) | async-done | bytes 2359328 | tf_op jit(solution)/shard_map/all_to_all | solution.py:70
  149.6 2.1 copy.255
  155.0 2.2 add_convert_fusion
  157.4 21.8 %all-gather.14 = f32[8,129,128]{2,1,0:T(8,128)S(1)} all-gather(f32[1,129,128]{2,1,0:T(8,128)S(1)} %maximum_bitcast_fusion.1), channel_id=4, replica_groups=mesh['sp_0'=8,'sp_1'=4,'sp_2'=2,'tp'=4] {'sp_0'}, dimensions={0}, use_global_device_ids=true | all-gather | bytes 594432 | tf_op jit(solution)/shard_map/all_gather | solution.py:28
  179.2 20.9 %all-gather.17 = f32[8,129,128]{2,1,0:T(8,128)S(1)} all-gather(f32[1,129,128]{2,1,0:T(8,128)S(1)} %maximum_bitcast_fusion.3), channel_id=7, replica_groups=mesh['sp_0'=8,'sp_1'=4,'sp_2'=2,'tp'=4] {'sp_0'}, dimensions={0}, use_global_device_ids=true | all-gather | bytes 594432 | tf_op jit(solution)/shard_map/all_gather | solution.py:28
  204.3 2.4 reduce-window.24
  216.1 3.3 reduce-window.26
  232.1 2.2 reshape.1346
  234.4 20.6 %all-to-all-start.2 = ((bf16[64,9,512]{2,1,0:T(8,128)(2,1)}), bf16[64,9,512]{2,1,0:T(8,128)(2,1)}, u32[]{:S(2)}, u32[]{:S(2)}) async-start(bf16[64,9,512]{2,1,0:T(8,128)(2,1)} %reshape.1346), calls=%async_computation.3 | async-start | bytes 2097152 | tf_op jit(solution)/shard_map/all_to_all | solution.py:253
  256.5 2.0 fusion.170
  258.5 2.3 copy.217
  260.8 2.0 fusion.171
  262.7 2.3 copy.218
  265.0 4.0 fusion.172
  269.0 14.0 %all-to-all-done.2 = bf16[64,9,512]{2,1,0:T(8,128)(2,1)} async-done(((bf16[64,9,512]{2,1,0:T(8,128)(2,1)}), bf16[64,9,512]{2,1,0:T(8,128)(2,1)}, u32[]{:S(2)}, u32[]{:S(2)}) %all-to-all-start.2) | async-done | bytes 589856 | tf_op jit(solution)/shard_map/all_to_all | solution.py:253
  284.5 2.6 gather_fusion.2
  288.6 2.0 multiply_reduce_fusion
  291.6 11.2 %all_gather.75 = bf16[192,2048]{1,0:T(8,128)(2,1)S(1)} all-gather(bf16[192,512]{1,0:T(8,128)(2,1)S(1)} %add_convert_fusion.1), channel_id=1, replica_groups=mesh['sp_0'=8,'sp_1'=4,'sp_2'=2,'tp'=4] {'tp'}, dimensions={1}, use_global_device_ids=true | all-gather | bytes 983040 | tf_op jit(solution)/shard_map/all_gather | solution.py:260
  305.0 5.7 %all-gather.21 = f32[2,129,128]{2,1,0:T(8,128)S(1)} all-gather(f32[1,129,128]{2,1,0:T(8,128)S(1)} %fusion.205), channel_id=11, replica_groups=mesh['sp_0'=8,'sp_1'=4,'sp_2'=2,'tp'=4] {'sp_2'}, dimensions={0}, use_global_device_ids=true | all-gather | bytes 198144 | tf_op jit(solution)/shard_map/all_gather | solution.py:28
  312.1 10.1 %all-gather.22 = f32[4,129,128]{2,1,0:T(8,128)S(1)} all-gather(f32[1,129,128]{2,1,0:T(8,128)S(1)} %maximum_bitcast_fusion.6), channel_id=12, replica_groups=mesh['sp_0'=8,'sp_1'=4,'sp_2'=2,'tp'=4] {'sp_1'}, dimensions={0}, use_global_device_ids=true | all-gather | bytes 330240 | tf_op jit(solution)/shard_map/all_gather | solution.py:28
  323.6 19.7 %all-gather.23 = f32[8,129,128]{2,1,0:T(8,128)S(1)} all-gather(f32[1,129,128]{2,1,0:T(8,128)S(1)} %maximum_bitcast_fusion.7), channel_id=13, replica_groups=mesh['sp_0'=8,'sp_1'=4,'sp_2'=2,'tp'=4] {'sp_0'}, dimensions={0}, use_global_device_ids=true | all-gather | bytes 594432 | tf_op jit(solution)/shard_map/all_gather | solution.py:28
  345.0 10.6 %all-gather.18 = f32[2,129,128]{2,1,0:T(8,128)S(1)} all-gather(f32[1,129,128]{2,1,0:T(8,128)S(1)} %fusion.203), channel_id=8, replica_groups=mesh['sp_0'=8,'sp_1'=4,'sp_2'=2,'tp'=4] {'sp_2'}, dimensions={0}, use_global_device_ids=true | all-gather | bytes 198144 | tf_op jit(solution)/shard_map/all_gather | solution.py:28
  356.9 10.0 %all-gather.19 = f32[4,129,128]{2,1,0:T(8,128)S(1)} all-gather(f32[1,129,128]{2,1,0:T(8,128)S(1)} %maximum_bitcast_fusion.4), channel_id=9, replica_groups=mesh['sp_0'=8,'sp_1'=4,'sp_2'=2,'tp'=4] {'sp_1'}, dimensions={0}, use_global_device_ids=true | all-gather | bytes 330240 | tf_op jit(solution)/shard_map/all_gather | solution.py:28
  368.4 20.1 %all-gather.20 = f32[8,129,128]{2,1,0:T(8,128)S(1)} all-gather(f32[1,129,128]{2,1,0:T(8,128)S(1)} %maximum_bitcast_fusion.5), channel_id=10, replica_groups=mesh['sp_0'=8,'sp_1'=4,'sp_2'=2,'tp'=4] {'sp_0'}, dimensions={0}, use_global_device_ids=true | all-gather | bytes 594432 | tf_op jit(solution)/shard_map/all_gather | solution.py:28
  392.7 3.0 fusion.253
  396.1 13.9 %all-to-all-start.3 = ((f32[64,32,256]{2,1,0:T(8,128)}), f32[64,32,256]{2,1,0:T(8,128)}, u32[]{:S(2)}, u32[]{:S(2)}) async-start(f32[64,32,256]{2,1,0:T(8,128)} %fusion.253), calls=%async_computation.4 | async-start | bytes 4194304 | tf_op jit(solution)/shard_map/all_to_all | solution.py:93
  422.0 23.2 %while.112 = (s32[]{:T(128)}, f32[2,64,128]{2,1,0:T(8,128)S(1)}, f32[3,2,64,64]{3,2,1,0:T(8,128)S(1)}, f32[3,2,64,64]{3,2,1,0:T(8,128)S(1)}, f32[3,2,64,128]{3,2...) while((s32[]{:T(128)}, f32[2,64,128]{2,1,0:T(8,128)S(1)}, ...), condition=%wide.region_22.23_spmd.clone, body=%wide.region_21.22_spmd.clone.sunk | while | flops 14802947 | bytes 1518041 | solution.py:133
  449.0 24.9 %while.113 = (s32[]{:T(128)}, f32[2,64,128]{2,1,0:T(8,128)S(1)}, f32[3,2,64,64]{3,2,1,0:T(8,128)S(1)}, f32[3,2,64,64]{3,2,1,0:T(8,128)}, f32[3,2,64,128]{3,2,0,1...) while((s32[]{:T(128)}, f32[2,64,128]{2,1,0:T(8,128)S(1)}, ...), condition=%wide.region_24.25_spmd.clone, body=%wide.region_23.24_spmd.clone.sunk | while | flops 14802947 | bytes 1501393 | solution.py:133
  454.0 1.7 fusion.378
  462.3 1.7 fusion.378
  470.6 1.7 fusion.378
  474.5 1.7 copy.209
  476.2 1.7 copy.210
  478.6 1.7 copy.204
  487.4 2.3 reduce_sum.75
  (624 shorter events, 190.5 us)
Async XLA Ops:
  7.2 132.2 %copy-start = (bf16[1,576,2048]{2,1,0:T(8,128)(2,1)S(1)}, bf16[1,576,2048]{2,1,0:T(8,128)(2,1)}, u32[]{:S(2)}) copy-start(bf16[1,576,2048]{2,1,0:T(8,128)(2,1)} %param.24) | copy-start | bytes 7077892
  26.7 88.6 %all-to-all-start = ((bf16[64,9,512]{2,1,0:T(8,128)(2,1)}), bf16[64,9,512]{2,1,0:T(8,128)(2,1)}, u32[]{:S(2)}, u32[]{:S(2)}) async-start(bf16[64,9,512]{2,1,0:T(8,128)(2,1)} %multiply_convert_fusion), calls=%async_computation | async-start | bytes 2097152 | tf_op jit(solution)/shard_map/all_to_all | solution.py:213
  94.9 23.4 %copy-start.2 = (bf16[3,2,64,128]{3,2,1,0:T(8,128)(2,1)}, bf16[3,2,64,128]{3,2,1,0:T(8,128)(2,1)S(1)}, u32[]{:S(2)}) copy-start(bf16[3,2,64,128]{3,2,1,0:T(8,128)(2,1)S(1)} %get-tuple-element.2618) | copy-start | bytes 294916
  114.1 109.7 %copy-start.62 = (f32[2,64]{1,0:T(2,128)}, f32[2,64]{1,0:T(2,128)S(1)}, u32[]{:S(2)}) copy-start(f32[2,64]{1,0:T(2,128)S(1)} %squeeze.560) | copy-start | bytes 1540
  114.2 109.7 %copy-start.64 = (f32[2,64]{1,0:T(2,128)}, f32[2,64]{1,0:T(2,128)S(1)}, u32[]{:S(2)}) copy-start(f32[2,64]{1,0:T(2,128)S(1)} %squeeze.559) | copy-start | bytes 1540
  114.3 109.6 %copy-start.66 = (f32[2,64]{1,0:T(2,128)}, f32[2,64]{1,0:T(2,128)S(1)}, u32[]{:S(2)}) copy-start(f32[2,64]{1,0:T(2,128)S(1)} %squeeze.558) | copy-start | bytes 1540
  115.0 108.9 %copy-start.68 = (f32[2,64]{1,0:T(2,128)}, f32[2,64]{1,0:T(2,128)S(1)}, u32[]{:S(2)}) copy-start(f32[2,64]{1,0:T(2,128)S(1)} %squeeze.562) | copy-start | bytes 1540
  118.3 31.3 %all-to-all-start.1 = ((bf16[4,576,512]{2,1,0:T(8,128)(2,1)}), bf16[4,576,512]{2,1,0:T(8,128)(2,1)}, u32[]{:S(2)}, u32[]{:S(2)}) async-start(bf16[4,576,512]{2,1,0:T(8,128)(2,1)} %broadcast_in_dim.154), calls=%async_computation.1 | async-start | bytes 4718592 | tf_op jit(solution)/shard_map/all_to_all | solution.py:70
  122.9 109.2 %reduce-scatter.2.cloned.1.call-start = ((), (), s32[]{:S(2)}) async-start(), calls=%async_computation.5 | async-start | bytes 2949120 | tf_op jit(solution)/shard_map/reduce_scatter | solution.py:252
  157.2 46.5 %copy-start.16 = (f32[192,128]{0,1:T(8,128)S(1)}, f32[192,128]{0,1:T(8,128)}, u32[]{:S(2)}) copy-start(f32[192,128]{0,1:T(8,128)} %copy-done.15) | copy-start | bytes 294916
  157.2 51.9 %copy-start.116 = (f32[128]{0:T(128)S(1)}, f32[128]{0:T(128)}, u32[]{:S(2)}) copy-start(f32[128]{0:T(128)} %get-tuple-element.1529) | copy-start | bytes 1540
  157.2 66.6 %copy-start.61 = (s32[384]{0:T(512)S(1)}, s32[384]{0:T(512)}, u32[]{:S(2)}) copy-start(s32[384]{0:T(512)} %get-tuple-element.1545) | copy-start | bytes 4612
  157.2 66.7 %copy-start.91 = (f32[2,64]{1,0:T(2,128)S(1)}, f32[2,64]{1,0:T(2,128)}, u32[]{:S(2)}) copy-start(f32[2,64]{1,0:T(2,128)} %squeeze.557) | copy-start | bytes 1540
  157.2 66.7 %copy-start.92 = (f32[2,64]{1,0:T(2,128)S(1)}, f32[2,64]{1,0:T(2,128)}, u32[]{:S(2)}) copy-start(f32[2,64]{1,0:T(2,128)} %squeeze.561) | copy-start | bytes 1540
  231.1 25.4 %copy-start.47 = (bf16[2,64,128]{2,1,0:T(8,128)(2,1)}, bf16[2,64,128]{2,1,0:T(8,128)(2,1)S(1)}, u32[]{:S(2)}) copy-start(bf16[2,64,128]{2,1,0:T(8,128)(2,1)S(1)} %add_add_fusion.4) | copy-start | bytes 98308
  231.1 23.8 %copy-start.71 = (f32[2,64]{1,0:T(2,128)S(1)}, f32[2,64]{1,0:T(2,128)}, u32[]{:S(2)}) copy-start(f32[2,64]{1,0:T(2,128)} %copy-done.70) | copy-start | bytes 1540
  231.1 23.8 %copy-start.73 = (f32[2,64]{1,0:T(2,128)S(1)}, f32[2,64]{1,0:T(2,128)}, u32[]{:S(2)}) copy-start(f32[2,64]{1,0:T(2,128)} %copy-done.72) | copy-start | bytes 1540
  231.1 23.8 %copy-start.75 = (f32[2,64]{1,0:T(2,128)S(1)}, f32[2,64]{1,0:T(2,128)}, u32[]{:S(2)}) copy-start(f32[2,64]{1,0:T(2,128)} %copy-done.74) | copy-start | bytes 1540
  231.2 23.8 %copy-start.77 = (f32[2,64]{1,0:T(2,128)S(1)}, f32[2,64]{1,0:T(2,128)}, u32[]{:S(2)}) copy-start(f32[2,64]{1,0:T(2,128)} %copy-done.76) | copy-start | bytes 1540
  231.2 23.8 %copy-start.78 = (f32[2,64]{1,0:T(2,128)S(1)}, f32[2,64]{1,0:T(2,128)}, u32[]{:S(2)}) copy-start(f32[2,64]{1,0:T(2,128)} %get-tuple-element.1699) | copy-start | bytes 1540
  231.2 23.8 %copy-start.79 = (f32[2,64]{1,0:T(2,128)S(1)}, f32[2,64]{1,0:T(2,128)}, u32[]{:S(2)}) copy-start(f32[2,64]{1,0:T(2,128)} %get-tuple-element.1700) | copy-start | bytes 1540
  231.2 23.8 %copy-start.80 = (f32[2,64]{1,0:T(2,128)S(1)}, f32[2,64]{1,0:T(2,128)}, u32[]{:S(2)}) copy-start(f32[2,64]{1,0:T(2,128)} %get-tuple-element.1843) | copy-start | bytes 1540
  231.2 23.8 %copy-start.81 = (f32[2,64]{1,0:T(2,128)S(1)}, f32[2,64]{1,0:T(2,128)}, u32[]{:S(2)}) copy-start(f32[2,64]{1,0:T(2,128)} %get-tuple-element.1844) | copy-start | bytes 1540
  232.1 22.9 %copy-start.56 = (f32[1,128,128]{2,1,0:T(8,128)S(1)}, f32[1,128,128]{2,1,0:T(8,128)}, u32[]{:S(2)}) copy-start(f32[1,128,128]{2,1,0:T(8,128)} %get-tuple-element.1756) | copy-start | bytes 196612
  232.1 22.9 %copy-start.57 = (f32[1,128,128]{2,1,0:T(8,128)S(1)}, f32[1,128,128]{2,1,0:T(8,128)}, u32[]{:S(2)}) copy-start(f32[1,128,128]{2,1,0:T(8,128)} %get-tuple-element.1757) | copy-start | bytes 196612
  232.1 24.4 %copy-start.9 = (bf16[576,256]{1,0:T(8,128)(2,1)S(1)}, bf16[576,256]{1,0:T(8,128)(2,1)}, u32[]{:S(2)}) copy-start(bf16[576,256]{1,0:T(8,128)(2,1)} %copy-done.8) | copy-start | bytes 884740
  234.4 48.6 %all-to-all-start.2 = ((bf16[64,9,512]{2,1,0:T(8,128)(2,1)}), bf16[64,9,512]{2,1,0:T(8,128)(2,1)}, u32[]{:S(2)}, u32[]{:S(2)}) async-start(bf16[64,9,512]{2,1,0:T(8,128)(2,1)} %reshape.1346), calls=%async_computation.3 | async-start | bytes 2097152 | tf_op jit(solution)/shard_map/all_to_all | solution.py:253
  256.5 46.7 %copy-start.45 = (bf16[2,64,128]{2,1,0:T(8,128)(2,1)}, bf16[2,64,128]{2,1,0:T(8,128)(2,1)S(1)}, u32[]{:S(2)}) copy-start(bf16[2,64,128]{2,1,0:T(8,128)(2,1)S(1)} %add_add_fusion.3) | copy-start | bytes 98308
  304.8 40.2 %copy-start.4 = (bf16[2,192,128]{2,1,0:T(8,128)(2,1)}, bf16[2,192,128]{2,1,0:T(8,128)(2,1)S(1)}, u32[]{:S(2)}) copy-start(bf16[2,192,128]{2,1,0:T(8,128)(2,1)S(1)} %add_add_fusion) | copy-start | bytes 294916
  304.8 40.2 %copy-start.83 = (f32[1,128]{1,0:T(1,128)S(1)}, f32[1,128]{1,0:T(1,128)}, u32[]{:S(2)}) copy-start(f32[1,128]{1,0:T(1,128)} %copy-done.82) | copy-start | bytes 1540
  345.0 44.9 %copy-start.5 = (bf16[2,192,128]{2,1,0:T(8,128)(2,1)S(1)}, bf16[2,192,128]{2,1,0:T(8,128)(2,1)}, u32[]{:S(2)}) copy-start(bf16[2,192,128]{2,1,0:T(8,128)(2,1)} %copy-done.4) | copy-start | bytes 294916
  366.9 25.7 %copy-start.44 = (bf16[192,2,128]{2,0,1:T(8,128)(2,1)S(1)}, bf16[192,2,128]{2,0,1:T(8,128)(2,1)}, u32[]{:S(2)}) copy-start(bf16[192,2,128]{2,0,1:T(8,128)(2,1)} %fusion.197) | copy-start | bytes 294916
  396.0 22.5 %copy-start.105 = (f32[128]{0:T(128)S(1)}, f32[128]{0:T(128)}, u32[]{:S(2)}) copy-start(f32[128]{0:T(128)} %get-tuple-element.1502) | copy-start | bytes 1540
  396.0 23.1 %copy-start.104 = (f32[128]{0:T(128)S(1)}, f32[128]{0:T(128)}, u32[]{:S(2)}) copy-start(f32[128]{0:T(128)} %get-tuple-element.1495) | copy-start | bytes 1540
  396.0 23.7 %copy-start.43 = (bf16[2,192,128]{2,1,0:T(8,128)(2,1)S(1)}, bf16[2,192,128]{2,1,0:T(8,128)(2,1)}, u32[]{:S(2)}) copy-start(bf16[2,192,128]{2,1,0:T(8,128)(2,1)} %rev.41) | copy-start | bytes 294916
  396.0 23.7 %copy-start.49 = (f32[1,128,128]{2,1,0:T(8,128)S(1)}, f32[1,128,128]{2,1,0:T(8,128)}, u32[]{:S(2)}) copy-start(f32[1,128,128]{2,1,0:T(8,128)} %get-tuple-element.1743) | copy-start | bytes 196612
  396.0 23.7 %copy-start.50 = (f32[1,128,128]{2,1,0:T(8,128)S(1)}, f32[1,128,128]{2,1,0:T(8,128)}, u32[]{:S(2)}) copy-start(f32[1,128,128]{2,1,0:T(8,128)} %get-tuple-element.1744) | copy-start | bytes 196612
  396.0 23.7 %copy-start.51 = (f32[1,128,128]{2,1,0:T(8,128)S(1)}, f32[1,128,128]{2,1,0:T(8,128)}, u32[]{:S(2)}) copy-start(f32[1,128,128]{2,1,0:T(8,128)} %get-tuple-element.1745) | copy-start | bytes 196612
  396.0 23.7 %copy-start.52 = (f32[1,128,128]{2,1,0:T(8,128)S(1)}, f32[1,128,128]{2,1,0:T(8,128)}, u32[]{:S(2)}) copy-start(f32[1,128,128]{2,1,0:T(8,128)} %get-tuple-element.1746) | copy-start | bytes 196612
  396.0 23.7 %copy-start.53 = (f32[1,128,128]{2,1,0:T(8,128)S(1)}, f32[1,128,128]{2,1,0:T(8,128)}, u32[]{:S(2)}) copy-start(f32[1,128,128]{2,1,0:T(8,128)} %get-tuple-element.1747) | copy-start | bytes 196612
  396.0 23.7 %copy-start.54 = (f32[1,128,128]{2,1,0:T(8,128)S(1)}, f32[1,128,128]{2,1,0:T(8,128)}, u32[]{:S(2)}) copy-start(f32[1,128,128]{2,1,0:T(8,128)} %get-tuple-element.1748) | copy-start | bytes 196612
  396.0 23.7 %copy-start.55 = (f32[1,128,128]{2,1,0:T(8,128)S(1)}, f32[1,128,128]{2,1,0:T(8,128)}, u32[]{:S(2)}) copy-start(f32[1,128,128]{2,1,0:T(8,128)} %get-tuple-element.1749) | copy-start | bytes 196612
  396.1 91.3 %all-to-all-start.3 = ((f32[64,32,256]{2,1,0:T(8,128)}), f32[64,32,256]{2,1,0:T(8,128)}, u32[]{:S(2)}, u32[]{:S(2)}) async-start(f32[64,32,256]{2,1,0:T(8,128)} %fusion.253), calls=%async_computation.4 | async-start | bytes 4194304 | tf_op jit(solution)/shard_map/all_to_all | solution.py:93
  422.0 23.9 %copy-start.48 = (f32[1,128,128]{2,1,0:T(8,128)S(1)}, f32[1,128,128]{2,1,0:T(8,128)}, u32[]{:S(2)}) copy-start(f32[1,128,128]{2,1,0:T(8,128)} %get-tuple-element.1735) | copy-start | bytes 196612
  422.0 27.0 %copy-start.3 = (bf16[3,2,64,128]{3,2,1,0:T(8,128)(2,1)S(1)}, bf16[3,2,64,128]{3,2,1,0:T(8,128)(2,1)}, u32[]{:S(2)}) copy-start(bf16[3,2,64,128]{3,2,1,0:T(8,128)(2,1)} %copy-done.2) | copy-start | bytes 294916
  448.9 33.0 %copy-start.14 = (f32[2,256,64]{1,2,0:T(8,128)S(1)}, f32[2,256,64]{1,2,0:T(8,128)}, u32[]{:S(2)}) copy-start(f32[2,256,64]{1,2,0:T(8,128)} %reverse.7) | copy-start | bytes 393220
  449.0 33.0 %copy-start.46 = (bf16[2,64,128]{2,1,0:T(8,128)(2,1)S(1)}, bf16[2,64,128]{2,1,0:T(8,128)(2,1)}, u32[]{:S(2)}) copy-start(bf16[2,64,128]{2,1,0:T(8,128)(2,1)} %copy-done.45) | copy-start | bytes 98308
  449.0 33.2 %copy-start.19 = (f32[2,256,64]{1,2,0:T(8,128)S(1)}, f32[2,256,64]{1,2,0:T(8,128)}, u32[]{:S(2)}) copy-start(f32[2,256,64]{1,2,0:T(8,128)} %copy-done.17) | copy-start | bytes 393220
  (79 other events, 933.6 us)
Sparse Core Ops, SparseCore 0:
  157.3 35.1 reduce-scatter.1
where the time goes:
time: 502 us; the launch traced here: 497 us
  blocking collectives  157 us (31%)
  local copies, waits for them, and re-layouts  119 us (24%)
  matrix products  84.1 us (17%)
  starting transfers between devices  52.6 us (10%)
  other arithmetic  47.3 us (9%)
  waiting for transfers between devices  19.6 us (4%)
  between operations  16 us (3%)
    all_gather x12, blocking collectives, all_in_one(): both, at, found = (lax.all_gather(jnp.concatenate(lines), axis), 0, {})  146 us
    unnamed x272, local copies, waits for them, and re-layouts  24 us
    dot_general x18, matrix products, advance(): jnp.einsum('hik,hjk->hij', query_block * jnp.exp(running_total - middle),...  21 us
    all_to_all x1, starting transfers between devices, on_device(): lax.all_to_all(summed.reshape(devices, capacity, quarter), SP, split_axis...  20.6 us
    dot_general x18, matrix products, advance(): jnp.einsum('zuw,zwo->zuo', query_block * jnp.exp(running_total), carried_...  16.4 us
    mul x32, local copies, waits for them, and re-layouts, combine(): return (earlier[0] * later[0], later[0][:, :, None] * earlier[1] + later[1])  15.3 us
    all_to_all x1, waiting for transfers between devices, on_device(): lax.all_to_all(summed.reshape(devices, capacity, quarter), SP, split_axis...  14 us
    all_to_all x1, starting transfers between devices, sum_at_owner(): lax.all_to_all(pieces, axis, split_axis=0, concat_axis=0, tiled=True)  13.9 us
  transfers between devices with their start and end apart: 5, of which 2 were waited for; matrix products, arithmetic and copies ran while one was open for 38% of the time, Pallas kernels for 0%

commit v1 on v0

--- a/solution.py
+++ b/solution.py
@@ -257,7 +257,10 @@
     moe_grad = jnp.sum(picked.reshape(rows_here, 2, quarter), axis=1)
     own_columns = lax.dynamic_slice_in_dim(layer_grad, lax.axis_index("tp") * quarter, quarter, 1)
     stream_part = (own_columns.astype(jnp.float32) + moe_grad).astype(jnp.bfloat16)
-    stream_grad = lax.all_gather(stream_part, "tp", axis=1, tiled=True)
+    view_terms = lambda shard_in: jnp.concatenate(
+        jax.lax.all_to_all(jnp.stack([shard_in] * jax.lax.axis_size("tp")), "tp", 0, 0), axis=1
+    )
+    stream_grad = view_terms(stream_part)
     scale = KEY_CHANNELS ** (-0.5)
 
     def split_heads(array, size):

time: 502 us -> 538 us (1.072)
  local copies, waits for them, and re-layouts: 119 us -> 152 us
  other arithmetic: 47.3 us -> 62.1 us
  blocking collectives: 157 us -> 143 us
  starting transfers between devices: 52.6 us -> 60.8 us
  waiting for transfers between devices: 19.6 us -> 11.5 us
    all_to_all x1, waiting for transfers between devices: 14 us -> 0.01 us  [on_device(): lax.all_to_all(summed.reshape(devices, capacity, quarter), SP, split_axis...]
    mul x32, local copies, waits for them, and re-layouts: 15.3 us -> 26.9 us  [combine(): return (earlier[0] * later[0], later[0][:, :, None] * earlier[1] + later[1])]
    all_gather x1 -> x0, blocking collectives: 11.2 us -> none  [on_device(): stream_grad = lax.all_gather(stream_part, 'tp', axis=1, tiled=True)]
    squeeze x24, local copies, waits for them, and re-layouts: 6.05 us -> 15.9 us  [carried_in(): total = combine(total, jax.tree.map(lambda part: part[k], pieces))]
    another operation x25 -> x26, local copies, waits for them, and re-layouts: 12.7 us -> 15.7 us
    unnamed x272 -> x218, local copies, waits for them, and re-layouts: 24 us -> 21.8 us
  transfers between devices with their start and end apart: 5 -> 6, of which waited for: 2 -> 2; matrix products, arithmetic and copies ran while one was open for 38% -> 43% of each run, Pallas kernels for 0% -> 0%
where the time goes in v1:
time: 538 us; the launch traced here: 533 us
  local copies, waits for them, and re-layouts  152 us (28%)
  blocking collectives  143 us (27%)
  matrix products  87.6 us (16%)
  other arithmetic  62.1 us (12%)
  starting transfers between devices  60.8 us (11%)
  between operations  15.4 us (3%)
  waiting for transfers between devices  11.5 us (2%)
    all_gather x12, blocking collectives, all_in_one(): both, at, found = (lax.all_gather(jnp.concatenate(lines), axis), 0, {})  143 us
    mul x32, local copies, waits for them, and re-layouts, combine(): return (earlier[0] * later[0], later[0][:, :, None] * earlier[1] + later[1])  26.9 us
    all_to_all x1, starting transfers between devices, on_device(): lax.all_to_all(summed.reshape(devices, capacity, quarter), SP, split_axis...  22.1 us
    unnamed x218, local copies, waits for them, and re-layouts  21.8 us
    dot_general x18, matrix products, advance(): jnp.einsum('hik,hjk->hij', query_block * jnp.exp(running_total - middle),...  21 us
    all_to_all x1, starting transfers between devices, sum_at_owner(): lax.all_to_all(pieces, axis, split_axis=0, concat_axis=0, tiled=True)  17 us
    dot_general x18, matrix products, advance(): jnp.einsum('zuw,zwo->zuo', query_block * jnp.exp(running_total), carried_...  16.4 us
    squeeze x24, local copies, waits for them, and re-layouts, carried_in(): total = combine(total, jax.tree.map(lambda part: part[k], pieces))  15.9 us
  transfers between devices with their start and end apart: 6, of which 2 were waited for; matrix products, arithmetic and copies ran while one was open for 43% of the time, Pallas kernels for 0%

profile of v1, /device:TPU:1, one launch (start us, length us, event | category | flops | bytes accessed | tf_op | source)
XLA Modules:
  0.0 532.6 jit_solution(18075352572923379351)
XLA Ops:
  11.3 2.9 scatter_custom_fusion
  15.2 2.7 gather_fusion
  19.8 4.0 gather_fusion.1
  23.9 2.8 multiply_convert_fusion
  26.7 13.5 %all-to-all-start = ((bf16[64,9,512]{2,1,0:T(8,128)(2,1)}), bf16[64,9,512]{2,1,0:T(8,128)(2,1)}, u32[]{:S(2)}, u32[]{:S(2)}) async-start(bf16[64,9,512]{2,1,0:T(8,128)(2,1)} %multiply_convert_fusion), calls=%async_computation | async-start | bytes 2097152 | tf_op jit(solution)/shard_map/all_to_all | solution.py:213
  57.8 17.1 %while.115 = (s32[]{:T(128)}, f32[2,64,128]{2,1,0:T(8,128)S(1)}, f32[3,2,64,128]{3,2,1,0:T(8,128)}, f32[3,2,64,64]{3,2,1,0:T(8,128)}, f32[3,2,64,64]{3,2,1,0:T(8...) while((s32[]{:T(128)}, f32[2,64,128]{2,1,0:T(8,128)S(1)}, ...), condition=%wide.region_11.12_spmd.clone, body=%wide.region_9.11_spmd.clone.sunk | while | flops 8093699 | bytes 2081263 | solution.py:133
  82.1 12.8 %while.114 = (s32[]{:T(128)}, f32[2,64,128]{2,1,0:T(8,128)S(1)}, f32[3,2,64,128]{3,2,1,0:T(8,128)}, f32[3,2,64,64]{3,2,1,0:T(8,128)}, f32[3,2,64,64]{3,2,1,0:T(8...) while((s32[]{:T(128)}, f32[2,64,128]{2,1,0:T(8,128)S(1)}, ...), condition=%wide.region_8.9_spmd.clone, body=%wide.region_6.8_spmd.clone.sunk | while | flops 8093699 | bytes 1981671 | solution.py:133
  98.1 2.1 reduce-window.24
  100.2 2.2 all-gather.12
  105.5 4.6 all-to-all-start.1
  110.2 1.9 all-gather.15
  112.8 11.1 %all-gather.13 = f32[4,129,128]{2,1,0:T(8,128)S(1)} all-gather(f32[1,129,128]{2,1,0:T(8,128)S(1)} %maximum_bitcast_fusion), channel_id=3, replica_groups=mesh['sp_0'=8,'sp_1'=4,'sp_2'=2,'tp'=4] {'sp_1'}, dimensions={0}, use_global_device_ids=true | all-gather | bytes 330240 | tf_op jit(solution)/shard_map/all_gather | solution.py:28
  125.4 2.9 fusion.175
  130.0 9.1 %all-to-all-done.1 = bf16[4,576,512]{2,1,0:T(8,128)(2,1)} async-done(((bf16[4,576,512]{2,1,0:T(8,128)(2,1)}), bf16[4,576,512]{2,1,0:T(8,128)(2,1)}, u32[]{:S(2)}, u32[]{:S(2)}) %all-to-all-start.1) | async-done | bytes 2359328 | tf_op jit(solution)/shard_map/all_to_all | solution.py:70
  139.1 2.1 copy.257
  144.5 2.2 add_convert_fusion
  148.5 2.9 rev.39
  159.7 11.2 %all-gather.16 = f32[4,129,128]{2,1,0:T(8,128)S(1)} all-gather(f32[1,129,128]{2,1,0:T(8,128)S(1)} %maximum_bitcast_fusion.2), channel_id=6, replica_groups=mesh['sp_0'=8,'sp_1'=4,'sp_2'=2,'tp'=4] {'sp_1'}, dimensions={0}, use_global_device_ids=true | all-gather | bytes 330240 | tf_op jit(solution)/shard_map/all_gather | solution.py:28
  181.5 3.3 reduce-window.26
  201.0 21.1 %all-gather.14 = f32[8,129,128]{2,1,0:T(8,128)S(1)} all-gather(f32[1,129,128]{2,1,0:T(8,128)S(1)} %maximum_bitcast_fusion.1), channel_id=4, replica_groups=mesh['sp_0'=8,'sp_1'=4,'sp_2'=2,'tp'=4] {'sp_0'}, dimensions={0}, use_global_device_ids=true | all-gather | bytes 594432 | tf_op jit(solution)/shard_map/all_gather | solution.py:28
  222.1 20.2 %all-gather.17 = f32[8,129,128]{2,1,0:T(8,128)S(1)} all-gather(f32[1,129,128]{2,1,0:T(8,128)S(1)} %maximum_bitcast_fusion.3), channel_id=7, replica_groups=mesh['sp_0'=8,'sp_1'=4,'sp_2'=2,'tp'=4] {'sp_0'}, dimensions={0}, use_global_device_ids=true | all-gather | bytes 594432 | tf_op jit(solution)/shard_map/all_gather | solution.py:28
  245.4 2.2 reshape.1353
  247.6 22.1 %all-to-all-start.2 = ((bf16[64,9,512]{2,1,0:T(8,128)(2,1)}), bf16[64,9,512]{2,1,0:T(8,128)(2,1)}, u32[]{:S(2)}, u32[]{:S(2)}) async-start(bf16[64,9,512]{2,1,0:T(8,128)(2,1)} %reshape.1353), calls=%async_computation.3 | async-start | bytes 2097152 | tf_op jit(solution)/shard_map/all_to_all | solution.py:253
  272.1 2.3 copy.227
  297.1 2.2 add_add_fusion.3
  299.4 2.0 fusion.170
  301.3 2.3 copy.219
  305.1 2.6 gather_fusion.2
  309.1 1.9 multiply_reduce_fusion
  313.0 3.5 all-to-all-start.3
  316.5 2.9 fusion.171
  319.5 2.3 copy.220
  321.7 4.0 fusion.172
  325.8 2.4 all-to-all-done.3
  329.7 2.8 reshape.1477
  332.5 2.0 convolution_bitcast_fusion
  337.1 3.2 all-gather.21
  341.6 10.5 %all-gather.22 = f32[4,129,128]{2,1,0:T(8,128)S(1)} all-gather(f32[1,129,128]{2,1,0:T(8,128)S(1)} %maximum_bitcast_fusion.6), channel_id=12, replica_groups=mesh['sp_0'=8,'sp_1'=4,'sp_2'=2,'tp'=4] {'sp_1'}, dimensions={0}, use_global_device_ids=true | all-gather | bytes 330240 | tf_op jit(solution)/shard_map/all_gather | solution.py:28
  353.6 21.1 %all-gather.23 = f32[8,129,128]{2,1,0:T(8,128)S(1)} all-gather(f32[1,129,128]{2,1,0:T(8,128)S(1)} %maximum_bitcast_fusion.7), channel_id=13, replica_groups=mesh['sp_0'=8,'sp_1'=4,'sp_2'=2,'tp'=4] {'sp_0'}, dimensions={0}, use_global_device_ids=true | all-gather | bytes 594432 | tf_op jit(solution)/shard_map/all_gather | solution.py:28
  376.4 9.8 %all-gather.18 = f32[2,129,128]{2,1,0:T(8,128)S(1)} all-gather(f32[1,129,128]{2,1,0:T(8,128)S(1)} %fusion.200), channel_id=8, replica_groups=mesh['sp_0'=8,'sp_1'=4,'sp_2'=2,'tp'=4] {'sp_2'}, dimensions={0}, use_global_device_ids=true | all-gather | bytes 198144 | tf_op jit(solution)/shard_map/all_gather | solution.py:28
  387.6 10.0 %all-gather.19 = f32[4,129,128]{2,1,0:T(8,128)S(1)} all-gather(f32[1,129,128]{2,1,0:T(8,128)S(1)} %maximum_bitcast_fusion.4), channel_id=9, replica_groups=mesh['sp_0'=8,'sp_1'=4,'sp_2'=2,'tp'=4] {'sp_1'}, dimensions={0}, use_global_device_ids=true | all-gather | bytes 330240 | tf_op jit(solution)/shard_map/all_gather | solution.py:28
  399.0 20.4 %all-gather.20 = f32[8,129,128]{2,1,0:T(8,128)S(1)} all-gather(f32[1,129,128]{2,1,0:T(8,128)S(1)} %maximum_bitcast_fusion.5), channel_id=10, replica_groups=mesh['sp_0'=8,'sp_1'=4,'sp_2'=2,'tp'=4] {'sp_0'}, dimensions={0}, use_global_device_ids=true | all-gather | bytes 594432 | tf_op jit(solution)/shard_map/all_gather | solution.py:28
  423.2 2.2 copy.172
  425.6 3.0 fusion.250
  428.9 17.0 %all-to-all-start.4 = ((f32[64,32,256]{2,1,0:T(8,128)}), f32[64,32,256]{2,1,0:T(8,128)}, u32[]{:S(2)}, u32[]{:S(2)}) async-start(f32[64,32,256]{2,1,0:T(8,128)} %fusion.250), calls=%async_computation.5 | async-start | bytes 4194304 | tf_op jit(solution)/shard_map/all_to_all | solution.py:93
  458.1 23.2 %while.112 = (s32[]{:T(128)}, f32[2,64,128]{2,1,0:T(8,128)S(1)}, f32[3,2,64,64]{3,2,1,0:T(8,128)S(1)}, f32[3,2,64,64]{3,2,1,0:T(8,128)S(1)}, f32[3,2,64,128]{3,2...) while((s32[]{:T(128)}, f32[2,64,128]{2,1,0:T(8,128)S(1)}, ...), condition=%wide.region_22.23_spmd.clone, body=%wide.region_21.22_spmd.clone.sunk | while | flops 14802947 | bytes 1518041 | solution.py:133
  485.1 24.9 %while.113 = (s32[]{:T(128)}, f32[2,64,128]{2,1,0:T(8,128)S(1)}, f32[3,2,64,64]{3,2,1,0:T(8,128)S(1)}, f32[3,2,64,64]{3,2,1,0:T(8,128)}, f32[3,2,64,128]{3,2,0,1...) while((s32[]{:T(128)}, f32[2,64,128]{2,1,0:T(8,128)S(1)}, ...), condition=%wide.region_24.25_spmd.clone, body=%wide.region_23.24_spmd.clone.sunk | while | flops 14802947 | bytes 1501393 | solution.py:133
  523.5 2.3 reduce_sum.75
  (576 shorter events, 237.1 us)
Async XLA Ops:
  7.2 118.2 %copy-start = (bf16[1,576,2048]{2,1,0:T(8,128)(2,1)S(1)}, bf16[1,576,2048]{2,1,0:T(8,128)(2,1)}, u32[]{:S(2)}) copy-start(bf16[1,576,2048]{2,1,0:T(8,128)(2,1)} %param.24) | copy-start | bytes 7077892
  26.7 75.8 %all-to-all-start = ((bf16[64,9,512]{2,1,0:T(8,128)(2,1)}), bf16[64,9,512]{2,1,0:T(8,128)(2,1)}, u32[]{:S(2)}, u32[]{:S(2)}) async-start(bf16[64,9,512]{2,1,0:T(8,128)(2,1)} %multiply_convert_fusion), calls=%async_computation | async-start | bytes 2097152 | tf_op jit(solution)/shard_map/all_to_all | solution.py:213
  105.5 33.6 %all-to-all-start.1 = ((bf16[4,576,512]{2,1,0:T(8,128)(2,1)}), bf16[4,576,512]{2,1,0:T(8,128)(2,1)}, u32[]{:S(2)}, u32[]{:S(2)}) async-start(bf16[4,576,512]{2,1,0:T(8,128)(2,1)} %broadcast_in_dim.154), calls=%async_computation.1 | async-start | bytes 4718592 | tf_op jit(solution)/shard_map/all_to_all | solution.py:70
  110.1 135.3 %reduce-scatter.2.cloned.1.call-start = ((), (), s32[]{:S(2)}) async-start(), calls=%async_computation.6 | async-start | bytes 2949120 | tf_op jit(solution)/shard_map/reduce_scatter | solution.py:252
  199.3 46.0 %copy-start.30 = (f32[2,192,128]{2,1,0:T(8,128)S(1)}, f32[2,192,128]{2,1,0:T(8,128)}, u32[]{:S(2)}) copy-start(f32[2,192,128]{2,1,0:T(8,128)} %rev.39) | copy-start | bytes 589828
  199.3 46.0 %copy-start.31 = (f32[2,3,64,128]{3,2,1,0:T(8,128)S(1)}, f32[2,3,64,128]{3,2,1,0:T(8,128)}, u32[]{:S(2)}) copy-start(f32[2,3,64,128]{3,2,1,0:T(8,128)} %copy.184) | copy-start | bytes 589828
  245.3 26.0 %copy-start.52 = (f32[384]{0:T(512)S(1)}, f32[384]{0:T(512)}, u32[]{:S(2)}) copy-start(f32[384]{0:T(512)} %compare_convert_fusion) | copy-start | bytes 4612
  247.6 46.1 %copy-start.34 = (f32[2,256,64]{1,2,0:T(8,128)S(1)}, f32[2,256,64]{1,2,0:T(8,128)}, u32[]{:S(2)}) copy-start(f32[2,256,64]{1,2,0:T(8,128)} %bitcast_bitcast_fusion) | copy-start | bytes 393220
  247.6 46.9 %copy-start.53 = (s32[384]{0:T(512)S(1)}, s32[384]{0:T(512)}, u32[]{:S(2)}) copy-start(s32[384]{0:T(512)} %get-tuple-element.1545) | copy-start | bytes 4612
  247.6 47.0 %copy-start.57 = (f32[2,64]{1,0:T(2,128)S(1)}, f32[2,64]{1,0:T(2,128)}, u32[]{:S(2)}) copy-start(f32[2,64]{1,0:T(2,128)} %squeeze.560) | copy-start | bytes 1540
  247.6 47.0 %copy-start.58 = (f32[2,64]{1,0:T(2,128)S(1)}, f32[2,64]{1,0:T(2,128)}, u32[]{:S(2)}) copy-start(f32[2,64]{1,0:T(2,128)} %squeeze.559) | copy-start | bytes 1540
  247.6 48.6 %copy-start.11 = (f32[2,256,64]{1,2,0:T(8,128)S(1)}, f32[2,256,64]{1,2,0:T(8,128)}, u32[]{:S(2)}) copy-start(f32[2,256,64]{1,2,0:T(8,128)} %bitcast_bitcast_fusion.1) | copy-start | bytes 393220
  247.6 56.0 %all-to-all-start.2 = ((bf16[64,9,512]{2,1,0:T(8,128)(2,1)}), bf16[64,9,512]{2,1,0:T(8,128)(2,1)}, u32[]{:S(2)}, u32[]{:S(2)}) async-start(bf16[64,9,512]{2,1,0:T(8,128)(2,1)} %reshape.1353), calls=%async_computation.3 | async-start | bytes 2097152 | tf_op jit(solution)/shard_map/all_to_all | solution.py:253
  269.7 27.4 %copy-start.54 = (f32[2,64]{1,0:T(2,128)S(1)}, f32[2,64]{1,0:T(2,128)}, u32[]{:S(2)}) copy-start(f32[2,64]{1,0:T(2,128)} %squeeze.586) | copy-start | bytes 1540
  269.7 27.4 %copy-start.55 = (f32[2,64]{1,0:T(2,128)S(1)}, f32[2,64]{1,0:T(2,128)}, u32[]{:S(2)}) copy-start(f32[2,64]{1,0:T(2,128)} %squeeze.585) | copy-start | bytes 1540
  269.8 27.4 %copy-start.56 = (f32[2,64]{1,0:T(2,128)S(1)}, f32[2,64]{1,0:T(2,128)}, u32[]{:S(2)}) copy-start(f32[2,64]{1,0:T(2,128)} %squeeze.584) | copy-start | bytes 1540
  269.8 27.4 %copy-start.59 = (f32[2,64]{1,0:T(2,128)S(1)}, f32[2,64]{1,0:T(2,128)}, u32[]{:S(2)}) copy-start(f32[2,64]{1,0:T(2,128)} %squeeze.588) | copy-start | bytes 1540
  313.0 15.1 %all-to-all-start.3 = ((bf16[4,192,512]{2,1,0:T(8,128)(2,1)}), bf16[4,192,512]{2,1,0:T(8,128)(2,1)S(1)}, u32[]{:S(2)}, u32[]{:S(2)}) async-start(bf16[4,192,512]{2,1,0:T(8,128)(2,1)} %stack.2), calls=%async_computation.4 | async-start | bytes 1572864 | tf_op jit(solution)/shard_map/all_to_all | solution.py:261
  336.7 39.4 %copy-start.8 = (f32[2,256,64]{1,2,0:T(8,128)S(1)}, f32[2,256,64]{1,2,0:T(8,128)}, u32[]{:S(2)}) copy-start(f32[2,256,64]{1,2,0:T(8,128)} %reverse.7) | copy-start | bytes 393220
  336.9 39.4 %copy-start.4 = (bf16[2,192,128]{2,1,0:T(8,128)(2,1)}, bf16[2,192,128]{2,1,0:T(8,128)(2,1)S(1)}, u32[]{:S(2)}) copy-start(bf16[2,192,128]{2,1,0:T(8,128)(2,1)S(1)} %add_add_fusion) | copy-start | bytes 294916
  336.9 39.4 %copy-start.61 = (f32[1,128]{1,0:T(1,128)S(1)}, f32[1,128]{1,0:T(1,128)}, u32[]{:S(2)}) copy-start(f32[1,128]{1,0:T(1,128)} %copy-done.60) | copy-start | bytes 1540
  376.4 44.5 %copy-start.5 = (bf16[2,192,128]{2,1,0:T(8,128)(2,1)S(1)}, bf16[2,192,128]{2,1,0:T(8,128)(2,1)}, u32[]{:S(2)}) copy-start(bf16[2,192,128]{2,1,0:T(8,128)(2,1)} %copy-done.4) | copy-start | bytes 294916
  428.7 23.8 %copy-start.91 = (f32[128]{0:T(128)S(1)}, f32[128]{0:T(128)}, u32[]{:S(2)}) copy-start(f32[128]{0:T(128)} %get-tuple-element.1524) | copy-start | bytes 1540
  428.7 23.9 %copy-start.90 = (f32[128]{0:T(128)S(1)}, f32[128]{0:T(128)}, u32[]{:S(2)}) copy-start(f32[128]{0:T(128)} %get-tuple-element.1525) | copy-start | bytes 1540
  428.8 23.9 %copy-start.71 = (f32[128]{0:T(128)S(1)}, f32[128]{0:T(128)}, u32[]{:S(2)}) copy-start(f32[128]{0:T(128)} %get-tuple-element.1540) | copy-start | bytes 1540
  428.8 24.0 %copy-start.69 = (f32[128]{0:T(128)S(1)}, f32[128]{0:T(128)}, u32[]{:S(2)}) copy-start(f32[128]{0:T(128)} %get-tuple-element.1539) | copy-start | bytes 1540
  428.8 24.1 %copy-start.85 = (f32[128]{0:T(128)S(1)}, f32[128]{0:T(128)}, u32[]{:S(2)}) copy-start(f32[128]{0:T(128)} %get-tuple-element.1496) | copy-start | bytes 1540
  428.8 24.2 %copy-start.84 = (f32[128]{0:T(128)S(1)}, f32[128]{0:T(128)}, u32[]{:S(2)}) copy-start(f32[128]{0:T(128)} %get-tuple-element.1497) | copy-start | bytes 1540
  428.8 24.2 %copy-start.83 = (f32[128]{0:T(128)S(1)}, f32[128]{0:T(128)}, u32[]{:S(2)}) copy-start(f32[128]{0:T(128)} %get-tuple-element.1498) | copy-start | bytes 1540
  428.8 24.3 %copy-start.82 = (f32[128]{0:T(128)S(1)}, f32[128]{0:T(128)}, u32[]{:S(2)}) copy-start(f32[128]{0:T(128)} %get-tuple-element.1499) | copy-start | bytes 1540
  428.8 24.4 %copy-start.81 = (f32[128]{0:T(128)S(1)}, f32[128]{0:T(128)}, u32[]{:S(2)}) copy-start(f32[128]{0:T(128)} %get-tuple-element.1500) | copy-start | bytes 1540
  428.8 25.0 %copy-start.80 = (f32[128]{0:T(128)S(1)}, f32[128]{0:T(128)}, u32[]{:S(2)}) copy-start(f32[128]{0:T(128)} %get-tuple-element.1501) | copy-start | bytes 1540
  428.8 25.7 %copy-start.79 = (f32[128]{0:T(128)S(1)}, f32[128]{0:T(128)}, u32[]{:S(2)}) copy-start(f32[128]{0:T(128)} %get-tuple-element.1502) | copy-start | bytes 1540
  428.8 26.3 %copy-start.78 = (f32[128]{0:T(128)S(1)}, f32[128]{0:T(128)}, u32[]{:S(2)}) copy-start(f32[128]{0:T(128)} %get-tuple-element.1495) | copy-start | bytes 1540
  428.9 26.9 %copy-start.35 = (bf16[2,192,128]{2,1,0:T(8,128)(2,1)S(1)}, bf16[2,192,128]{2,1,0:T(8,128)(2,1)}, u32[]{:S(2)}) copy-start(bf16[2,192,128]{2,1,0:T(8,128)(2,1)} %rev.41) | copy-start | bytes 294916
  428.9 27.0 %copy-start.41 = (f32[1,128,128]{2,1,0:T(8,128)S(1)}, f32[1,128,128]{2,1,0:T(8,128)}, u32[]{:S(2)}) copy-start(f32[1,128,128]{2,1,0:T(8,128)} %get-tuple-element.1743) | copy-start | bytes 196612
  428.9 27.0 %copy-start.42 = (f32[1,128,128]{2,1,0:T(8,128)S(1)}, f32[1,128,128]{2,1,0:T(8,128)}, u32[]{:S(2)}) copy-start(f32[1,128,128]{2,1,0:T(8,128)} %get-tuple-element.1744) | copy-start | bytes 196612
  428.9 27.0 %copy-start.43 = (f32[1,128,128]{2,1,0:T(8,128)S(1)}, f32[1,128,128]{2,1,0:T(8,128)}, u32[]{:S(2)}) copy-start(f32[1,128,128]{2,1,0:T(8,128)} %get-tuple-element.1745) | copy-start | bytes 196612
  428.9 27.0 %copy-start.44 = (f32[1,128,128]{2,1,0:T(8,128)S(1)}, f32[1,128,128]{2,1,0:T(8,128)}, u32[]{:S(2)}) copy-start(f32[1,128,128]{2,1,0:T(8,128)} %get-tuple-element.1746) | copy-start | bytes 196612
  428.9 27.0 %copy-start.45 = (f32[1,128,128]{2,1,0:T(8,128)S(1)}, f32[1,128,128]{2,1,0:T(8,128)}, u32[]{:S(2)}) copy-start(f32[1,128,128]{2,1,0:T(8,128)} %get-tuple-element.1747) | copy-start | bytes 196612
  428.9 27.0 %copy-start.46 = (f32[1,128,128]{2,1,0:T(8,128)S(1)}, f32[1,128,128]{2,1,0:T(8,128)}, u32[]{:S(2)}) copy-start(f32[1,128,128]{2,1,0:T(8,128)} %get-tuple-element.1748) | copy-start | bytes 196612
  428.9 27.0 %copy-start.47 = (f32[1,128,128]{2,1,0:T(8,128)S(1)}, f32[1,128,128]{2,1,0:T(8,128)}, u32[]{:S(2)}) copy-start(f32[1,128,128]{2,1,0:T(8,128)} %get-tuple-element.1749) | copy-start | bytes 196612
  428.9 94.5 %all-to-all-start.4 = ((f32[64,32,256]{2,1,0:T(8,128)}), f32[64,32,256]{2,1,0:T(8,128)}, u32[]{:S(2)}, u32[]{:S(2)}) async-start(f32[64,32,256]{2,1,0:T(8,128)} %fusion.250), calls=%async_computation.5 | async-start | bytes 4194304 | tf_op jit(solution)/shard_map/all_to_all | solution.py:93
  458.1 23.9 %copy-start.40 = (f32[1,128,128]{2,1,0:T(8,128)S(1)}, f32[1,128,128]{2,1,0:T(8,128)}, u32[]{:S(2)}) copy-start(f32[1,128,128]{2,1,0:T(8,128)} %get-tuple-element.1735) | copy-start | bytes 196612
  458.1 27.0 %copy-start.3 = (bf16[3,2,64,128]{3,2,1,0:T(8,128)(2,1)S(1)}, bf16[3,2,64,128]{3,2,1,0:T(8,128)(2,1)}, u32[]{:S(2)}) copy-start(bf16[3,2,64,128]{3,2,1,0:T(8,128)(2,1)} %copy-done.2) | copy-start | bytes 294916
  485.0 33.0 %copy-start.9 = (f32[2,256,64]{1,2,0:T(8,128)S(1)}, f32[2,256,64]{1,2,0:T(8,128)}, u32[]{:S(2)}) copy-start(f32[2,256,64]{1,2,0:T(8,128)} %reverse.7) | copy-start | bytes 393220
  485.0 33.0 %copy-start.38 = (bf16[2,64,128]{2,1,0:T(8,128)(2,1)S(1)}, bf16[2,64,128]{2,1,0:T(8,128)(2,1)}, u32[]{:S(2)}) copy-start(bf16[2,64,128]{2,1,0:T(8,128)(2,1)} %add_add_fusion.3) | copy-start | bytes 98308
  485.0 33.2 %copy-start.13 = (f32[2,256,64]{1,2,0:T(8,128)S(1)}, f32[2,256,64]{1,2,0:T(8,128)}, u32[]{:S(2)}) copy-start(f32[2,256,64]{1,2,0:T(8,128)} %bitcast_bitcast_fusion.1) | copy-start | bytes 393220
  (53 other events, 577.6 us)
Sparse Core Ops, SparseCore 0:
  146.8 34.0 reduce-scatter.1
